TPU v7x, 32 devices: a whole 2x2x4 slice. The times are simulated.
32 devices in a mesh: fs: 16 (over z, y, x), tp: 2 (over core).
Axes of the slice: x: 2, y: 2, z: 4, core: 2. Of those that a mesh axis runs over, the one named last changes fastest.
Arguments:
- tokens: bfloat16 [4096, 2048], P('fs'), may hold values from -6 to 6
- mix_gain: float32 [2048], replicated, may hold values from 0.1 to 1.9
- glu_value: bfloat16 [2048, 2048], P('fs', 'tp'), may hold values from -0.125 to 0.125
- glu_gate: bfloat16 [2048, 2048], P('fs', 'tp'), may hold values from -0.125 to 0.125
- conv_taps: float32 [31, 2048], P(None, 'tp'), may hold values from -2.2 to 2.2, as said below
- chan_gain: float32 [2048], P('tp'), may hold values from 0.1 to 1.9
- mix_out: bfloat16 [2048, 2048], P('tp', 'fs'), may hold values from -0.125 to 0.125
- mlp_gain: float32 [2048], replicated, may hold values from 0.1 to 1.9
- up_weight: bfloat16 [2048, 8192], P('fs', 'tp'), may hold values from -0.125 to 0.125
- down_weight: bfloat16 [8192, 2048], P('tp', 'fs'), may hold values from -0.0625 to 0.0625
Outputs:
- result: bfloat16 [4096, 2048], P('fs')
Inputs may be any that keep to these rules, and one draw needn't show every extreme that they name: `conv_taps`: independent entries scaled by fan-in; channels fall into 16 groups of different scale.
All inputs are finite; a program needn't handle non-finite values.
Results may differ from a plain program's by a relative error of at most 0.018.
Values may be sent and summed in bfloat16 or wider, within the bound.
No kernel may reach another device: no remote copies, remote signals or barrier semaphores. Data moves between devices by JAX's collectives and lax.ppermute only.
A program may use at most 128 MiB of HBM per device.

v0:
```python
import jax
import jax.numpy as jnp
from jax import lax
from jax.sharding import PartitionSpec as P

C = 2048
LEN = 128
norm_floor = 0.05


def rms_scale(stream, gain):
    return stream * lax.rsqrt(jnp.mean(stream * stream, axis=-1, keepdims=True) + norm_floor) * gain


def bf16_round(value):
    return lax.optimization_barrier(value.astype(jnp.bfloat16)).astype(jnp.float32)


def depthwise(glu, conv_taps):
    seqs = glu.shape[0] // LEN
    blocks = glu.reshape(seqs, LEN, glu.shape[1]).astype(jnp.float32)
    reach = conv_taps.shape[0] // 2
    padded = jnp.pad(blocks, ((0, 0), (reach, reach), (0, 0)))
    total = jnp.zeros_like(blocks)
    for offset in range(conv_taps.shape[0]):
        total = total + padded[:, offset : offset + LEN] * conv_taps[offset]
    return total.reshape(glu.shape)


def per_device(
    tokens,
    mix_gain,
    glu_value,
    glu_gate,
    conv_taps,
    chan_gain,
    mix_out,
    mlp_gain,
    up_weight,
    down_weight,
):
    stream = tokens.astype(jnp.float32)
    normed = rms_scale(stream, mix_gain).astype(jnp.bfloat16)
    values = jnp.dot(
        normed,
        lax.all_gather(glu_value, "fs", axis=0, tiled=True),
        preferred_element_type=jnp.float32,
    )
    gating = jnp.dot(
        normed,
        lax.all_gather(glu_gate, "fs", axis=0, tiled=True),
        preferred_element_type=jnp.float32,
    )
    glu = (values * jax.nn.sigmoid(gating)).astype(jnp.bfloat16)
    convolved = depthwise(glu, conv_taps)
    sums, squares = lax.psum(
        (jnp.sum(convolved, axis=-1), jnp.sum(convolved * convolved, axis=-1)), "tp"
    )
    centre = (sums / C)[:, None]
    spread = (squares / C)[:, None] - centre * centre
    hidden = jax.nn.silu((convolved - centre) * lax.rsqrt(spread + norm_floor) * chan_gain).astype(
        jnp.bfloat16
    )
    whole_out = lax.all_gather(mix_out, "fs", axis=1, tiled=True)
    own_rows = stream.shape[0] // lax.axis_size("tp")
    mixed = lax.psum_scatter(
        jnp.dot(hidden, whole_out, preferred_element_type=jnp.float32).astype(jnp.bfloat16),
        "tp",
        scatter_dimension=0,
        tiled=True,
    ).astype(jnp.float32)
    own_stream = lax.dynamic_slice_in_dim(stream, lax.axis_index("tp") * own_rows, own_rows, 0)
    resid = own_stream + bf16_round(mixed)
    normed_mlp = rms_scale(resid, mlp_gain).astype(jnp.bfloat16)
    whole_up = lax.all_gather(up_weight, "fs", axis=0, tiled=True)
    active = jnp.square(
        jax.nn.relu(
            jnp.dot(
                lax.all_gather(normed_mlp, "tp", axis=0, tiled=True),
                whole_up,
                preferred_element_type=jnp.float32,
            )
        )
    ).astype(jnp.bfloat16)
    whole_down = lax.all_gather(down_weight, "fs", axis=1, tiled=True)
    feed = lax.psum_scatter(
        jnp.dot(active, whole_down, preferred_element_type=jnp.float32).astype(jnp.bfloat16),
        "tp",
        scatter_dimension=0,
        tiled=True,
    ).astype(jnp.float32)
    finished = (resid + bf16_round(feed)).astype(jnp.bfloat16)
    return lax.all_gather(finished, "tp", axis=0, tiled=True)


def solution(mesh):
    in_specs = (
        P("fs", None),
        P(),
        P("fs", "tp"),
        P("fs", "tp"),
        P(None, "tp"),
        P("tp"),
        P("tp", "fs"),
        P(),
        P("fs", "tp"),
        P("tp", "fs"),
    )
    out_specs = P("fs", None)
    return jax.shard_map(
        per_device, mesh=mesh, in_specs=in_specs, out_specs=out_specs, check_vma=False
    )
```

profile of v0, /device:TPU:0, one launch (start us, length us, event | category | flops | bytes accessed | tf_op | source)
XLA Modules:
  0.0 769.7 jit_solution(15755725362399529471)
XLA Ops:
  6.5 0.7 all-gather.10.cloned.1.call-update
  7.3 0.7 all-gather.8.cloned.1.call-update
  8.8 1.5 multiply_reduce_fusion
  10.3 1.1 fusion.72
  11.4 1.4 fusion.71
  12.9 75.6 %all-gather.10.cloned.1.call-done = bf16[2048,1024]{1,0:T(8,128)(2,1)} async-done(((bf16[128,1024]{1,0:T(8,128)(2,1)}), bf16[2048,1024]{1,0:T(8,128)(2,1)}) %all-gather.10.cloned.1.call-update) | async-done | bytes 4194320 | tf_op jit(solution)/shard_map/all_gather | solution.py:51
  88.4 3.9 fusion.4
  92.4 73.1 %all-gather.8.cloned.1.call-done = bf16[2048,1024]{1,0:T(8,128)(2,1)} async-done(((bf16[128,1024]{1,0:T(8,128)(2,1)}), bf16[2048,1024]{1,0:T(8,128)(2,1)}) %all-gather.8.cloned.1.call-update) | async-done | bytes 4194320 | tf_op jit(solution)/shard_map/all_gather | solution.py:46
  165.4 3.5 bitcast_convert_fusion
  169.0 5.7 fusion.69
  174.7 2.5 all-reduce.1
  177.6 77.9 %all-gather.12.cloned.1.call-done = bf16[1024,2048]{1,0:T(8,128)(2,1)} async-done(((bf16[1024,128]{1,0:T(8,128)(2,1)}), bf16[1024,2048]{1,0:T(8,128)(2,1)}) %all-gather.12.cloned.1.call-update) | async-done | bytes 4194320 | tf_op jit(solution)/shard_map/all_gather | solution.py:64
  255.5 4.4 convolution_convert_fusion.1
  260.2 6.4 reduce-scatter.3.cloned.1.call-done
  266.7 1.3 multiply_reduce_fusion.1
  267.9 2.0 multiply_convert_fusion.1
  271.4 9.0 %all-gather.14.cloned.1.call-done = bf16[256,2048]{1,0:T(8,128)(2,1)} async-done(((bf16[128,2048]{1,0:T(8,128)(2,1)}), bf16[256,2048]{1,0:T(8,128)(2,1)}) %all-gather.14.cloned.1.call-update) | async-done | bytes 1048592 | tf_op jit(solution)/shard_map/all_gather | solution.py:79
  280.4 194.8 %all-gather.16.cloned.1.call-done = bf16[2048,4096]{1,0:T(8,128)(2,1)} async-done(((bf16[128,4096]{1,0:T(8,128)(2,1)}), bf16[2048,4096]{1,0:T(8,128)(2,1)}) %all-gather.16.cloned.1.call-update) | async-done | bytes 16777232 | tf_op jit(solution)/shard_map/all_gather | solution.py:75
  475.2 250.0 %all-gather.18.cloned.1.call-done = bf16[4096,2048]{1,0:T(8,128)(2,1)} async-done(((bf16[4096,128]{1,0:T(8,128)(2,1)}), bf16[4096,2048]{1,0:T(8,128)(2,1)}) %all-gather.18.cloned.1.call-update) | async-done | bytes 16777232 | tf_op jit(solution)/shard_map/all_gather | solution.py:85
  725.2 16.4 %convolution_convert_fusion = bf16[256,2048]{1,0:T(8,128)(2,1)} fusion(bf16[4096,2048]{1,0:T(8,128)(2,1)} %all-gather.18.cloned.1.call-done, bf16[256,2048]{1,0:T(8,128)(2,1)} %all-gather.14.cloned.1.call-done, bf16[2048,4096]{1,0:T(8,128)(2,1)} %all-gather.16.cloned.1.call-done), kind=kOutput, calls=%fused_computation.33 | convolution fusion | flops 8593604608 | bytes 35651584 | tf_op jit(solution)/shard_map/dot_general | solution.py:87
  741.8 6.7 reduce-scatter.5.cloned.1.call-done
  748.4 2.0 add_convert_fusion
  750.5 10.4 %all-gather.20.cloned.1.call-done = bf16[256,2048]{1,0:T(8,128)(2,1)} async-done(((bf16[128,2048]{1,0:T(8,128)(2,1)}), bf16[256,2048]{1,0:T(8,128)(2,1)}) %all-gather.20.cloned.1.call-update) | async-done | bytes 1048592 | tf_op jit(solution)/shard_map/all_gather | solution.py:93
  760.9 2.3 copy.12
  (31 shorter events, 3.0 us)
Async XLA Ops:
  6.5 81.9 %all-gather.10.cloned.1.call-start = ((), (), s32[]{:S(2)}) async-start(), calls=%async_computation.3 | async-start | bytes 4456448 | tf_op jit(solution)/shard_map/all_gather | solution.py:51
  7.3 158.2 %all-gather.8.cloned.1.call-start = ((), (), s32[]{:S(2)}) async-start(), calls=%async_computation.2 | async-start | bytes 4456448 | tf_op jit(solution)/shard_map/all_gather | solution.py:46
  8.0 247.5 %all-gather.12.cloned.1.call-start = ((), (), s32[]{:S(2)}) async-start(), calls=%async_computation.4 | async-start | bytes 4456448 | tf_op jit(solution)/shard_map/all_gather | solution.py:64
  8.7 257.9 %reduce-scatter.3.cloned.1.call-start = ((), (), s32[]{:S(2)}) async-start(), calls=%async_computation.5 | async-start | bytes 1572864 | tf_op jit(solution)/shard_map/reduce_scatter | solution.py:66
  12.8 152.6 %copy-start.1 = (bf16[256,2048]{1,0:T(8,128)(2,1)S(1)}, bf16[256,2048]{1,0:T(8,128)(2,1)}, u32[]{:S(2)}) copy-start(bf16[256,2048]{1,0:T(8,128)(2,1)} %param.10) | copy-start | bytes 3145732
  12.8 152.6 %copy-start.4 = (f32[2048]{0:T(1024)S(1)}, f32[2048]{0:T(1024)}, u32[]{:S(2)}) copy-start(f32[2048]{0:T(1024)} %param.11) | copy-start | bytes 24580
  92.4 84.8 %copy-start.3 = (f32[1024]{0:T(1024)S(1)}, f32[1024]{0:T(1024)}, u32[]{:S(2)}) copy-start(f32[1024]{0:T(1024)} %param.15) | copy-start | bytes 12292
  259.9 8.0 %copy-start.2 = (f32[2048]{0:T(1024)S(1)}, f32[2048]{0:T(1024)}, u32[]{:S(2)}) copy-start(f32[2048]{0:T(1024)} %param.17) | copy-start | bytes 24580
  259.9 20.4 %all-gather.14.cloned.1.call-start = ((), (), s32[]{:S(2)}) async-start(), calls=%async_computation.6 | async-start | bytes 1572864 | tf_op jit(solution)/shard_map/all_gather | solution.py:79
  270.0 205.2 %all-gather.16.cloned.1.call-start = ((), (), s32[]{:S(2)}) async-start(), calls=%async_computation.7 | async-start | bytes 17825792 | tf_op jit(solution)/shard_map/all_gather | solution.py:75
  270.6 454.7 %all-gather.18.cloned.1.call-start = ((), (), s32[]{:S(2)}) async-start(), calls=%async_computation.8 | async-start | bytes 17825792 | tf_op jit(solution)/shard_map/all_gather | solution.py:85
  271.3 477.1 %copy-start = (bf16[128,2048]{1,0:T(8,128)(2,1)S(1)}, bf16[128,2048]{1,0:T(8,128)(2,1)}, u32[]{:S(2)}) copy-start(bf16[128,2048]{1,0:T(8,128)(2,1)} %reduce-scatter.3.cloned.1.call-done) | copy-start | bytes 1572868
  271.3 477.1 %reduce-scatter.5.cloned.1.call-start = ((), (), s32[]{:S(2)}) async-start(), calls=%async_computation.9 | async-start | bytes 1572864 | tf_op jit(solution)/shard_map/reduce_scatter | solution.py:86
  741.7 19.2 %all-gather.20.cloned.1.call-start = ((), (), s32[]{:S(2)}) async-start(), calls=%async_computation.10 | async-start | bytes 1572864 | tf_op jit(solution)/shard_map/all_gather | solution.py:93
Sparse Core Ops, SparseCore 0:
  10.1 78.3 all-gather.9
  91.2 74.1 all-gather.7
  168.1 87.3 all-gather.11
  260.1 6.5 reduce-scatter.2
  270.1 10.2 all-gather.13
  283.0 192.1 all-gather.15
  477.9 247.2 all-gather.17
  741.8 6.5 reduce-scatter.4
  750.6 10.2 all-gather.19
where the time goes:
time: 770 us
  waiting for transfers between devices  707 us (92%)
  matrix products  28.3 us (4%)
  between operations  13.3 us (2%)
  other arithmetic  13.2 us (2%)
    all_gather x1, waiting for transfers between devices, per_device(): whole_down = lax.all_gather(down_weight, 'fs', axis=1, tiled=True)  250 us
    all_gather x1, waiting for transfers between devices, per_device(): whole_up = lax.all_gather(up_weight, 'fs', axis=0, tiled=True)  195 us
    all_gather x1, waiting for transfers between devices, per_device(): whole_out = lax.all_gather(mix_out, 'fs', axis=1, tiled=True)  77.9 us
    all_gather x1, waiting for transfers between devices, per_device(): lax.all_gather(glu_gate, 'fs', axis=0, tiled=True)  75.6 us
    all_gather x1, waiting for transfers between devices, per_device(): lax.all_gather(glu_value, 'fs', axis=0, tiled=True)  73.1 us
    dot_general x1, matrix products, per_device(): jnp.dot(active, whole_down, preferred_element_type=jnp.float32)  16.4 us
  transfers between devices with their start and end apart: 9, of which 9 were waited for; matrix products, arithmetic and copies ran while one was open for 2% of the time, Pallas kernels for 0%

commit v1 on v0

--- a/solution.py
+++ b/solution.py
@@ -82,7 +82,7 @@
             )
         )
     ).astype(jnp.bfloat16)
-    whole_down = lax.all_gather(down_weight, "fs", axis=1, tiled=True)
+    whole_down = jnp.concatenate(lax.all_gather(down_weight, "fs"), axis=1)
     feed = lax.psum_scatter(
         jnp.dot(active, whole_down, preferred_element_type=jnp.float32).astype(jnp.bfloat16),
         "tp",

time: 770 us -> 711 us (0.923)
  waiting for transfers between devices: 707 us -> 626 us
  local copies, waits for them, and re-layouts: 4.85 us -> 25.6 us
    all_gather x1, waiting for transfers between devices: 250 us -> 191 us  [per_device(): whole_down = jnp.concatenate(lax.all_gather(down_weight, 'fs'), axis=1)]
    reshape x0 -> x1, local copies, waits for them, and re-layouts: none -> 20.8 us  [per_device(): whole_down = jnp.concatenate(lax.all_gather(down_weight, 'fs'), axis=1)]
    all_gather x1, waiting for transfers between devices: 195 us -> 183 us  [per_device(): whole_up = lax.all_gather(up_weight, 'fs', axis=0, tiled=True)]
    all_gather x1, waiting for transfers between devices: 9.01 us -> 0.01 us  [per_device(): lax.all_gather(normed_mlp, 'tp', axis=0, tiled=True)]
  transfers between devices with their start and end apart: 9 -> 9, of which waited for: 9 -> 8; matrix products, arithmetic and copies ran while one was open for 2% -> 6% of each run, Pallas kernels for 0% -> 0%
where the time goes in v1:
time: 711 us; the launch traced here: 710 us
  waiting for transfers between devices  626 us (88%)
  matrix products  28.3 us (4%)
  local copies, waits for them, and re-layouts  25.6 us (4%)
  between operations  13.3 us (2%)
  other arithmetic  13.2 us (2%)
    all_gather x1, waiting for transfers between devices, per_device(): whole_down = jnp.concatenate(lax.all_gather(down_weight, 'fs'), axis=1)  191 us
    all_gather x1, waiting for transfers between devices, per_device(): whole_up = lax.all_gather(up_weight, 'fs', axis=0, tiled=True)  183 us
    all_gather x1, waiting for transfers between devices, per_device(): whole_out = lax.all_gather(mix_out, 'fs', axis=1, tiled=True)  77.9 us
    all_gather x1, waiting for transfers between devices, per_device(): lax.all_gather(glu_gate, 'fs', axis=0, tiled=True)  75.6 us
    all_gather x1, waiting for transfers between devices, per_device(): lax.all_gather(glu_value, 'fs', axis=0, tiled=True)  73.1 us
    reshape x1, local copies, waits for them, and re-layouts, per_device(): whole_down = jnp.concatenate(lax.all_gather(down_weight, 'fs'), axis=1)  20.8 us
    dot_general x1, matrix products, per_device(): jnp.dot(active, whole_down, preferred_element_type=jnp.float32)  16.5 us
  transfers between devices with their start and end apart: 9, of which 8 were waited for; matrix products, arithmetic and copies ran while one was open for 6% of the time, Pallas kernels for 0%

profile of v1, /device:TPU:0, one launch (start us, length us, event | category | flops | bytes accessed | tf_op | source)
XLA Modules:
  0.0 709.7 jit_solution(16312465658057118294)
XLA Ops:
  6.5 0.7 all-gather.11.cloned.1.call-update
  7.3 0.7 all-gather.9.cloned.1.call-update
  8.8 1.5 multiply_reduce_fusion
  10.3 1.1 fusion.72
  11.4 1.4 fusion.71
  12.8 75.6 %all-gather.11.cloned.1.call-done = bf16[2048,1024]{1,0:T(8,128)(2,1)} async-done(((bf16[128,1024]{1,0:T(8,128)(2,1)}), bf16[2048,1024]{1,0:T(8,128)(2,1)}) %all-gather.11.cloned.1.call-update) | async-done | bytes 4194320 | tf_op jit(solution)/shard_map/all_gather | solution.py:51
  88.4 3.9 fusion.4
  92.4 73.1 %all-gather.9.cloned.1.call-done = bf16[2048,1024]{1,0:T(8,128)(2,1)} async-done(((bf16[128,1024]{1,0:T(8,128)(2,1)}), bf16[2048,1024]{1,0:T(8,128)(2,1)}) %all-gather.9.cloned.1.call-update) | async-done | bytes 4194320 | tf_op jit(solution)/shard_map/all_gather | solution.py:46
  165.4 3.5 bitcast_convert_fusion
  168.9 5.7 fusion.69
  174.6 2.5 all-reduce.1
  177.6 77.9 %all-gather.13.cloned.1.call-done = bf16[1024,2048]{1,0:T(8,128)(2,1)} async-done(((bf16[1024,128]{1,0:T(8,128)(2,1)}), bf16[1024,2048]{1,0:T(8,128)(2,1)}) %all-gather.13.cloned.1.call-update) | async-done | bytes 4194320 | tf_op jit(solution)/shard_map/all_gather | solution.py:64
  255.5 4.4 convolution_convert_fusion.1
  260.8 5.8 reduce-scatter.3.cloned.1.call-done
  266.7 1.3 multiply_reduce_fusion.1
  267.9 2.0 multiply_convert_fusion.1
  271.0 190.6 %all-gather.21.cloned.1.call-done = bf16[65536,128]{1,0:T(8,128)(2,1)} async-done(((bf16[4096,128]{1,0:T(8,128)(2,1)}), bf16[65536,128]{1,0:T(8,128)(2,1)}) %all-gather.21.cloned.1.call-update) | async-done | bytes 16777232 | tf_op jit(solution)/shard_map/all_gather | solution.py:85
  461.5 20.8 %copy.11 = bf16[4096,16,128]{0,2,1:T(8,128)(2,1)} copy(bf16[4096,16,128]{2,0,1:T(8,128)(2,1)} %bitcast.57) | data formatting | bytes 33554432 | tf_op jit(solution)/shard_map/reshape | solution.py:85
  482.3 182.8 %all-gather.17.cloned.1.call-done = bf16[2048,4096]{1,0:T(8,128)(2,1)} async-done(((bf16[128,4096]{1,0:T(8,128)(2,1)}), bf16[2048,4096]{1,0:T(8,128)(2,1)}) %all-gather.17.cloned.1.call-update) | async-done | bytes 16777232 | tf_op jit(solution)/shard_map/all_gather | solution.py:75
  665.1 16.5 %convolution_convert_fusion = bf16[256,2048]{1,0:T(8,128)(2,1)} fusion(bf16[4096,2048]{0,1:T(8,128)(2,1)} %bitcast.58, bf16[256,2048]{1,0:T(8,128)(2,1)} %all-gather.15.cloned.1.call-done, bf16[2048,4096]{1,0:T(8,128)(2,1)} %all-gather.17.cloned.1.call-done), kind=kOutput, calls=%fused_computation.33 | convolution fusion | flops 8593604608 | bytes 35651584 | tf_op jit(solution)/shard_map/dot_general | solution.py:87
  681.7 6.7 reduce-scatter.5.cloned.1.call-done
  688.4 2.0 add_convert_fusion
  690.5 10.4 %all-gather.19.cloned.1.call-done = bf16[256,2048]{1,0:T(8,128)(2,1)} async-done(((bf16[128,2048]{1,0:T(8,128)(2,1)}), bf16[256,2048]{1,0:T(8,128)(2,1)}) %all-gather.19.cloned.1.call-update) | async-done | bytes 1048592 | tf_op jit(solution)/shard_map/all_gather | solution.py:93
  700.9 2.3 copy.13
  (32 shorter events, 3.2 us)
Async XLA Ops:
  6.5 81.9 %all-gather.11.cloned.1.call-start = ((), (), s32[]{:S(2)}) async-start(), calls=%async_computation.3 | async-start | bytes 4456448 | tf_op jit(solution)/shard_map/all_gather | solution.py:51
  7.3 158.2 %all-gather.9.cloned.1.call-start = ((), (), s32[]{:S(2)}) async-start(), calls=%async_computation.2 | async-start | bytes 4456448 | tf_op jit(solution)/shard_map/all_gather | solution.py:46
  8.0 247.5 %all-gather.13.cloned.1.call-start = ((), (), s32[]{:S(2)}) async-start(), calls=%async_computation.4 | async-start | bytes 4456448 | tf_op jit(solution)/shard_map/all_gather | solution.py:64
  8.7 257.9 %reduce-scatter.3.cloned.1.call-start = ((), (), s32[]{:S(2)}) async-start(), calls=%async_computation.5 | async-start | bytes 1572864 | tf_op jit(solution)/shard_map/reduce_scatter | solution.py:66
  12.8 152.6 %copy-start.1 = (bf16[256,2048]{1,0:T(8,128)(2,1)S(1)}, bf16[256,2048]{1,0:T(8,128)(2,1)}, u32[]{:S(2)}) copy-start(bf16[256,2048]{1,0:T(8,128)(2,1)} %param.10) | copy-start | bytes 3145732
  12.8 152.6 %copy-start.4 = (f32[2048]{0:T(1024)S(1)}, f32[2048]{0:T(1024)}, u32[]{:S(2)}) copy-start(f32[2048]{0:T(1024)} %param.11) | copy-start | bytes 24580
  92.4 84.8 %copy-start.3 = (f32[1024]{0:T(1024)S(1)}, f32[1024]{0:T(1024)}, u32[]{:S(2)}) copy-start(f32[1024]{0:T(1024)} %param.15) | copy-start | bytes 12292
  259.9 8.0 %copy-start.2 = (f32[2048]{0:T(1024)S(1)}, f32[2048]{0:T(1024)}, u32[]{:S(2)}) copy-start(f32[2048]{0:T(1024)} %param.17) | copy-start | bytes 24580
  259.9 201.6 %all-gather.21.cloned.1.call-start = ((), (), s32[]{:S(2)}) async-start(), calls=%async_computation.10 | async-start | bytes 17825792 | tf_op jit(solution)/shard_map/all_gather | solution.py:85
  260.5 221.8 %all-gather.15.cloned.1.call-start = ((), (), s32[]{:S(2)}) async-start(), calls=%async_computation.6 | async-start | bytes 1572864 | tf_op jit(solution)/shard_map/all_gather | solution.py:79
  270.0 395.2 %all-gather.17.cloned.1.call-start = ((), (), s32[]{:S(2)}) async-start(), calls=%async_computation.7 | async-start | bytes 17825792 | tf_op jit(solution)/shard_map/all_gather | solution.py:75
  270.7 417.7 %reduce-scatter.5.cloned.1.call-start = ((), (), s32[]{:S(2)}) async-start(), calls=%async_computation.8 | async-start | bytes 1572864 | tf_op jit(solution)/shard_map/reduce_scatter | solution.py:86
  665.1 23.3 %copy-start = (bf16[128,2048]{1,0:T(8,128)(2,1)S(1)}, bf16[128,2048]{1,0:T(8,128)(2,1)}, u32[]{:S(2)}) copy-start(bf16[128,2048]{1,0:T(8,128)(2,1)} %reduce-scatter.3.cloned.1.call-done) | copy-start | bytes 1572868
  681.7 19.2 %all-gather.19.cloned.1.call-start = ((), (), s32[]{:S(2)}) async-start(), calls=%async_computation.9 | async-start | bytes 1572864 | tf_op jit(solution)/shard_map/all_gather | solution.py:93
Sparse Core Ops, SparseCore 0:
  10.1 78.3 all-gather.10
  91.2 74.1 all-gather.8
  168.1 87.3 all-gather.12
  260.1 6.5 reduce-scatter.2
  269.3 192.2 all-gather.20
  462.9 7.1 all-gather.14
  472.9 192.1 all-gather.16
  681.8 6.5 reduce-scatter.4
  690.6 10.2 all-gather.18
